TPU v7x, 32 devices: a whole 2x2x4 slice. The times are simulated.
32 devices in a mesh: sp: 16 (over z, y, x), tp: 2 (over core).
Axes of the slice: x: 2, y: 2, z: 4, core: 2. Of those that a mesh axis runs over, the one named last changes fastest.
Arguments:
- queries: bfloat16 [6144, 2048], P('sp', 'tp'), may hold values from -6 to 6
- key_heads: bfloat16 [6144, 1024], P('sp', 'tp'), may hold values from -6 to 6
- value_heads: bfloat16 [6144, 1024], P('sp', 'tp'), may hold values from -6 to 6
- sink_logit: float32 [16], P('tp'), may hold values from 3 to 7
- doc_ids: int32 [6144], replicated, may hold values from 0 to 3, never falling along the last dimension, each value on 1 to 3072 neighbouring positions
- residual: bfloat16 [6144, 2048], P('sp'), may hold values from -6 to 6
- out_proj: bfloat16 [2048, 2048], P('tp'), may hold values from -0.125 to 0.125
- gain_mix: float32 [2048], replicated, may hold values from 0.1 to 1.9
- up_proj: bfloat16 [2048, 8192], P('sp', 'tp'), may hold values from -0.125 to 0.125
- down_proj: bfloat16 [8192, 2048], P('tp', 'sp'), may hold values from -0.0625 to 0.0625
- gain_ffn_in: float32 [2048], replicated, may hold values from 0.1 to 1.9
- gain_ffn_out: float32 [2048], replicated, may hold values from 0.1 to 1.9
Outputs:
- layer_out: bfloat16 [6144, 2048], P(('sp', 'tp'))
All inputs are finite; a program needn't handle non-finite values.
Results may differ from a plain program's by a relative error of at most 0.019.
Values may be sent and summed in bfloat16 or wider, within the bound.
A program may use at most 128 MiB of HBM per device.

v0:
```python
import jax
import jax.numpy as jnp
from jax import lax
from jax.sharding import PartitionSpec as P

HD = 128
WINDOW = 128


def padded(shard, sides, width):
    for axis, dim in sides:
        devices, length = (lax.axis_size(axis), shard.shape[dim])
        up = [(i, (i + 1) % devices) for i in range(devices - 1)]
        down = [(j, i) for i, j in up]
        last = lax.slice_in_dim(shard, length - width, length, axis=dim)
        first = lax.slice_in_dim(shard, 0, width, axis=dim)
        before = lax.ppermute(last, axis, up)
        after = lax.ppermute(first, axis, down)
        shard = jnp.concatenate([before, shard, after], axis=dim)
    return shard


def rotate(field, places):
    half_dim = HD // 2
    inv_freq = 10000.0 ** (-jnp.arange(0, HD, 2, dtype=jnp.float32) / HD)
    angles = places[:, None, None] * inv_freq[None, None, :]
    cosine = jnp.cos(angles)
    sine = jnp.sin(angles)
    lower = field[..., :half_dim].astype(jnp.float32)
    upper = field[..., half_dim:].astype(jnp.float32)
    return jnp.concatenate(
        [lower * cosine - upper * sine, upper * cosine + lower * sine], axis=-1
    ).astype(jnp.bfloat16)


def banded(field, blocks):
    framed = field.reshape((blocks + 2, WINDOW) + field.shape[1:])
    return jnp.concatenate([framed[:-2], framed[1:-1], framed[2:]], axis=1)


def rms_scale(field, gain_vec):
    return field * lax.rsqrt(jnp.mean(field * field, axis=-1, keepdims=True) + 1e-06) * gain_vec


def body(
    queries,
    key_heads,
    value_heads,
    sink_logit,
    doc_ids,
    residual,
    out_proj,
    gain_mix,
    up_proj,
    down_proj,
    gain_ffn_in,
    gain_ffn_out,
):
    tok_count = queries.shape[0]
    blocks = tok_count // WINDOW
    share_rows = tok_count // lax.axis_size("tp")
    q_local = queries.shape[1] // HD
    kv_local = key_heads.shape[1] // HD
    group_size = q_local // kv_local
    offset = lax.axis_index("sp") * tok_count
    places = (offset + jnp.arange(tok_count)).astype(jnp.float32)
    rotated_q = rotate(queries.reshape(tok_count, q_local, HD), places).reshape(
        blocks, WINDOW, kv_local, group_size, HD
    )
    rotated_k = rotate(key_heads.reshape(tok_count, kv_local, HD), places).reshape(
        tok_count, kv_local * HD
    )
    rimmed = padded(jnp.stack([rotated_k, value_heads]), (("sp", 1),), WINDOW)
    key_win = banded(rimmed[0].reshape(-1, kv_local, HD), blocks)
    val_win = banded(rimmed[1].reshape(-1, kv_local, HD), blocks)
    padded_docs = jnp.pad(doc_ids, (WINDOW, WINDOW), constant_values=-1)
    key_docs = banded(lax.dynamic_slice_in_dim(padded_docs, offset, tok_count + 2 * WINDOW), blocks)
    query_docs = lax.dynamic_slice_in_dim(doc_ids, offset, tok_count).reshape(blocks, WINDOW)
    q_index = jnp.arange(WINDOW)[:, None]
    k_index = jnp.arange(3 * WINDOW)[None, :]
    in_window = jnp.abs(k_index - WINDOW - q_index) <= WINDOW
    allowed = (in_window[None] & (query_docs[:, :, None] == key_docs[:, None, :]))[:, None, None]
    scores = jnp.einsum(
        "nqkgd,nskd->nkgqs", rotated_q, key_win, preferred_element_type=jnp.float32
    ) * HD ** (-0.5)
    masked = jnp.where(allowed, scores, -1e30)
    sink_col = sink_logit.reshape(kv_local, group_size)[None, :, :, None]
    top_score = jnp.maximum(jnp.max(masked, axis=-1), sink_col)
    exp_scores = jnp.where(allowed, jnp.exp(masked - top_score[..., None]), 0.0)
    denom_sum = jnp.sum(exp_scores, axis=-1) + jnp.exp(sink_col - top_score)
    probs = (exp_scores / denom_sum[..., None]).astype(jnp.bfloat16)
    attn = (
        jnp.einsum("nkgqs,nskd->nqkgd", probs, val_win, preferred_element_type=jnp.float32)
        .astype(jnp.bfloat16)
        .reshape(tok_count, q_local * HD)
    )
    mixed = lax.psum(
        jnp.dot(attn, out_proj, preferred_element_type=jnp.float32).astype(jnp.bfloat16), "tp"
    ).astype(jnp.float32)
    after_all = (residual.astype(jnp.float32) + rms_scale(mixed, gain_mix)).astype(jnp.bfloat16)
    normed = rms_scale(after_all.astype(jnp.float32), gain_ffn_in).astype(jnp.bfloat16)
    after_mix = lax.dynamic_slice_in_dim(
        after_all, lax.axis_index("tp") * share_rows, share_rows, 0
    )
    up_acts = jnp.dot(
        normed,
        lax.all_gather(up_proj, "sp", axis=0, tiled=True),
        preferred_element_type=jnp.float32,
    )
    hidden = jnp.square(jax.nn.relu(up_acts)).astype(jnp.bfloat16)
    partial_value = jnp.dot(
        hidden,
        lax.all_gather(down_proj, "sp", axis=1, tiled=True),
        preferred_element_type=jnp.float32,
    )
    ffn_out = lax.psum_scatter(
        partial_value.astype(jnp.bfloat16), "tp", scatter_dimension=0, tiled=True
    ).astype(jnp.float32)
    return (after_mix.astype(jnp.float32) + rms_scale(ffn_out, gain_ffn_out)).astype(jnp.bfloat16)


def solution(mesh):
    return jax.shard_map(
        body,
        mesh=mesh,
        in_specs=(
            P("sp", "tp"),
            P("sp", "tp"),
            P("sp", "tp"),
            P("tp"),
            P(),
            P("sp", None),
            P("tp", None),
            P(),
            P("sp", "tp"),
            P("tp", "sp"),
            P(),
            P(),
        ),
        out_specs=P(("sp", "tp"), None),
        check_vma=False,
    )
```

profile of v0, /device:TPU:0, one launch (start us, length us, event | category | flops | bytes accessed | tf_op | source)
XLA Modules:
  0.0 535.9 jit_solution(408335233760002139)
XLA Ops:
  7.4 1.3 copy.28
  8.7 1.2 copy.29
  9.9 0.4 multiply_cosine_fusion
  10.3 0.1 fusion.41
  10.5 0.8 pad_maximum_fusion.7
  11.3 5.6 %collective-permute-start = (bf16[2,128,512]{1,2,0:T(8,128)(2,1)}, bf16[2,128,512]{1,2,0:T(8,128)(2,1)}, u32[]{:S(2)}, u32[]{:S(2)}) collective-permute-start(bf16[2,128,512]{1,2,0:T(8,128)(2,1)} %get-tuple-element.15), channel_id=1, source_target_pairs={{0,2},{2,4},{4,6},{6,8},{8,10},{10,12},{12,14},{14,16},{16,18},{18... | collective-permute-start | bytes 786440 | tf_op jit(solution)/shard_map/ppermute | solution.py:17
  16.9 1.3 collective-permute-start.1
  18.3 0.1 abs_compare_fusion
  18.4 0.4 copy.58
  18.8 0.3 fusion.35
  19.2 0.9 copy.36
  20.1 0.1 slice.109
  20.2 0.1 concatenate.36
  20.3 1.2 copy.43
  21.5 0.1 concatenate.37
  21.6 1.2 copy.44
  22.9 0.7 max.25
  23.6 1.0 copy.33
  24.5 0.2 compare_and_fusion
  24.8 2.9 collective-permute-done
  27.7 1.9 collective-permute-done.1
  29.6 1.3 pad_maximum_fusion.5
  30.9 0.1 reshape.208
  31.0 0.3 copy.38
  31.3 0.1 reshape.209
  31.5 0.3 copy.40
  31.8 2.4 fusion.1
  34.3 2.0 copy-done
  36.4 1.2 fusion.2
  37.6 0.1 exponential_add_fusion
  37.7 0.1 reshape.206
  37.9 0.1 reshape.207
  38.1 4.0 fusion.24
  42.0 0.6 copy.46
  42.7 0.6 reshape.203
  43.2 5.1 convolution_convert_fusion
  48.4 0.5 all-gather.3.cloned.1.call-update
  49.0 0.5 all-gather.5.cloned.1.call-update
  49.6 0.2 reduce-scatter.2.cloned.1.call-start
  49.8 19.4 %all-reduce.3.cloned.1.call-done = bf16[384,2048]{1,0:T(8,128)(2,1)} async-done(((bf16[384,2048]{1,0:T(8,128)(2,1)}), bf16[384,2048]{1,0:T(8,128)(2,1)}) %all-reduce.3.cloned.1.call-update) | async-done | bytes 1572880 | tf_op jit(solution)/shard_map/psum | solution.py:97
  69.2 1.8 fusion.3
  71.0 2.3 fusion.7
  73.3 169.4 %all-gather.3.cloned.1.call-done = bf16[2048,4096]{1,0:T(8,128)(2,1)} async-done(((bf16[128,4096]{1,0:T(8,128)(2,1)}), bf16[2048,4096]{1,0:T(8,128)(2,1)}) %all-gather.3.cloned.1.call-update) | async-done | bytes 16777232 | tf_op jit(solution)/shard_map/all_gather | solution.py:107
  242.7 249.7 %all-gather.5.cloned.1.call-done = bf16[4096,2048]{1,0:T(8,128)(2,1)} async-done(((bf16[4096,128]{1,0:T(8,128)(2,1)}), bf16[4096,2048]{1,0:T(8,128)(2,1)}) %all-gather.5.cloned.1.call-update) | async-done | bytes 16777232 | tf_op jit(solution)/shard_map/all_gather | solution.py:113
  492.4 24.9 %fusion.11 = bf16[384,2048]{1,0:T(8,128)(2,1)} fusion(bf16[4096,2048]{1,0:T(8,128)(2,1)} %all-gather.5.cloned.1.call-done, bf16[2048,4096]{1,0:T(8,128)(2,1)} %all-gather.3.cloned.1.call-done, bf16[384,2048]{1,0:T(8,128)(2,1)S(1)} %get-tuple-element.6, f32[2048]{0:T(1024)S(1)} %copy-done.11, f32[384]{0:T(512)S(1)} %add_rsqrt_fusion), kind=kOutput, calls=%fused_computation.19 | convolution fusion | flops 12893552640 | bytes 36709888 | tf_op jit(solution)/shard_map/dot_general | solution.py:111
  517.4 7.4 %reduce-scatter.2.cloned.1.call-done = bf16[192,2048]{1,0:T(8,128)(2,1)} async-done(((bf16[384,2048]{1,0:T(8,128)(2,1)}), bf16[192,2048]{1,0:T(8,128)(2,1)}) %reduce-scatter.2.cloned.1.call-update) | async-done | bytes 786448 | tf_op jit(solution)/shard_map/reduce_scatter | solution.py:116
  524.7 1.4 fusion.13
  526.1 2.4 fusion.16
  (42 shorter events, 0.7 us)
Async XLA Ops:
  7.4 10.8 %copy-start.6 = (s32[6144]{0:T(1024)S(1)}, s32[6144]{0:T(1024)}, u32[]{:S(2)}) copy-start(s32[6144]{0:T(1024)} %param.16) | copy-start | bytes 73732
  7.4 11.0 %copy-start.3 = (bf16[384,1024]{1,0:T(8,128)(2,1)S(1)}, bf16[384,1024]{1,0:T(8,128)(2,1)}, u32[]{:S(2)}) copy-start(bf16[384,1024]{1,0:T(8,128)(2,1)} %param.12) | copy-start | bytes 2359300
  7.4 61.8 %all-reduce.3.cloned.1.call-start = ((), (), s32[]{:S(2)}) async-start(), calls=%async_computation.1 | async-start | bytes 3145728 | tf_op jit(solution)/shard_map/psum | solution.py:97
  10.5 9.6 %copy-start.1 = (bf16[384,512]{1,0:T(8,128)(2,1)S(1)}, bf16[384,512]{1,0:T(8,128)(2,1)}, u32[]{:S(2)}) copy-start(bf16[384,512]{1,0:T(8,128)(2,1)} %param.14) | copy-start | bytes 1179652
  11.3 16.3 %collective-permute-start = (bf16[2,128,512]{1,2,0:T(8,128)(2,1)}, bf16[2,128,512]{1,2,0:T(8,128)(2,1)}, u32[]{:S(2)}, u32[]{:S(2)}) collective-permute-start(bf16[2,128,512]{1,2,0:T(8,128)(2,1)} %get-tuple-element.15), channel_id=1, source_target_pairs={{0,2},{2,4},{4,6},{6,8},{8,10},{10,12},{12,14},{14,16},{16,18},{18... | collective-permute-start | bytes 786440 | tf_op jit(solution)/shard_map/ppermute | solution.py:17
  16.9 12.7 %collective-permute-start.1 = (bf16[2,128,512]{1,2,0:T(8,128)(2,1)S(1)}, bf16[2,128,512]{1,2,0:T(8,128)(2,1)}, u32[]{:S(2)}, u32[]{:S(2)}) collective-permute-start(bf16[2,128,512]{1,2,0:T(8,128)(2,1)S(1)} %get-tuple-element.16), channel_id=1, source_target_pairs={{2,0},{4,2},{6,4},{8,6},{10,8},{12,10},{14,12},{16,14},{18,16},{20... | collective-permute-start | bytes 786440 | tf_op jit(solution)/shard_map/ppermute | solution.py:18
  19.0 3.8 copy-start.10
  24.7 7.0 %copy-start.4 = (bf16[3,128,4,2,64]{4,1,3,2,0:T(8,128)(2,1)S(1)}, bf16[3,128,4,2,64]{4,1,3,2,0:T(8,128)(2,1)}, u32[]{:S(2)}) copy-start(bf16[3,128,4,2,64]{4,1,3,2,0:T(8,128)(2,1)} %copy.43) | copy-start | bytes 1179652
  31.8 2.5 copy-start.7
  34.2 2.1 copy-start
  36.4 1.7 copy-start.5
  48.4 22.6 %copy-start.2 = (bf16[384,2048]{1,0:T(8,128)(2,1)S(1)}, bf16[384,2048]{1,0:T(8,128)(2,1)}, u32[]{:S(2)}) copy-start(bf16[384,2048]{1,0:T(8,128)(2,1)} %param.17) | copy-start | bytes 4718596
  48.4 22.6 %copy-start.8 = (f32[2048]{0:T(1024)S(1)}, f32[2048]{0:T(1024)}, u32[]{:S(2)}) copy-start(f32[2048]{0:T(1024)} %param.19) | copy-start | bytes 24580
  48.4 194.3 %all-gather.3.cloned.1.call-start = ((), (), s32[]{:S(2)}) async-start(), calls=%async_computation.2 | async-start | bytes 17825792 | tf_op jit(solution)/shard_map/all_gather | solution.py:107
  49.0 443.5 %all-gather.5.cloned.1.call-start = ((), (), s32[]{:S(2)}) async-start(), calls=%async_computation.3 | async-start | bytes 17825792 | tf_op jit(solution)/shard_map/all_gather | solution.py:113
  49.5 442.9 %copy-start.11 = (f32[2048]{0:T(1024)S(1)}, f32[2048]{0:T(1024)}, u32[]{:S(2)}) copy-start(f32[2048]{0:T(1024)} %param.22) | copy-start | bytes 24580
  49.6 475.2 %reduce-scatter.2.cloned.1.call-start = ((), (), s32[]{:S(2)}) async-start(), calls=%async_computation.4 | async-start | bytes 2359296 | tf_op jit(solution)/shard_map/reduce_scatter | solution.py:116
  492.4 33.7 %copy-start.9 = (f32[2048]{0:T(1024)S(1)}, f32[2048]{0:T(1024)}, u32[]{:S(2)}) copy-start(f32[2048]{0:T(1024)} %param.23) | copy-start | bytes 24580
Sparse Core Ops, SparseCore 0:
  48.5 20.6 all-reduce.2
  517.5 7.2 reduce-scatter.1
Sparse Core Ops, SparseCore 1:
  51.6 191.0 all-gather.2
  245.3 247.1 all-gather.4
where the time goes:
time: 536 us
  waiting for transfers between devices  452 us (84%)
  matrix products  36.4 us (7%)
  between operations  15.2 us (3%)
  local copies, waits for them, and re-layouts  12.9 us (2%)
  other arithmetic  12.5 us (2%)
  starting transfers between devices  7.15 us (1%)
    all_gather x1, waiting for transfers between devices, body(): lax.all_gather(down_proj, 'sp', axis=1, tiled=True)  250 us
    all_gather x1, waiting for transfers between devices, body(): lax.all_gather(up_proj, 'sp', axis=0, tiled=True)  169 us
    dot_general x1, matrix products, body(): jnp.dot(hidden, lax.all_gather(down_proj, 'sp', axis=1, tiled=True), pref...  24.9 us
    psum x1, waiting for transfers between devices, body(): lax.psum(jnp.dot(attn, out_proj, preferred_element_type=jnp.float32).asty...  19.4 us
  transfers between devices with their start and end apart: 6, of which 6 were waited for; matrix products, arithmetic and copies ran while one was open for 2% of the time, Pallas kernels for 0%

commit v1 on v0

--- a/solution.py
+++ b/solution.py
@@ -110,7 +110,7 @@
     hidden = jnp.square(jax.nn.relu(up_acts)).astype(jnp.bfloat16)
     partial_value = jnp.dot(
         hidden,
-        lax.all_gather(down_proj, "sp", axis=1, tiled=True),
+        jnp.concatenate(lax.all_gather(down_proj, axis_name="sp"), 1),
         preferred_element_type=jnp.float32,
     )
     ffn_out = lax.psum_scatter(

time: 536 us -> 473 us (0.88)
  waiting for transfers between devices: 452 us -> 372 us
  local copies, waits for them, and re-layouts: 12.9 us -> 34.3 us
  matrix products: 36.4 us -> 30.3 us
    all_gather x1, waiting for transfers between devices: 250 us -> 169 us  [body(): lax.all_gather(down_proj, axis_name='sp')]
    reshape x0 -> x1, local copies, waits for them, and re-layouts: none -> 21.4 us  [body(): jnp.concatenate(lax.all_gather(down_proj, axis_name='sp'), 1)]
    dot_general x1, matrix products: 24.9 us -> 18.8 us  [body(): jnp.dot(hidden, jnp.concatenate(lax.all_gather(down_proj, axis_name='sp')...]
  transfers between devices with their start and end apart: 6 -> 6, of which waited for: 6 -> 6; matrix products, arithmetic and copies ran while one was open for 2% -> 7% of each run, Pallas kernels for 0% -> 0%
where the time goes in v1:
time: 473 us; the launch traced here: 472 us
  waiting for transfers between devices  372 us (79%)
  local copies, waits for them, and re-layouts  34.3 us (7%)
  matrix products  30.3 us (6%)
  between operations  15.2 us (3%)
  other arithmetic  13.1 us (3%)
  starting transfers between devices  7.15 us (2%)
    all_gather x1, waiting for transfers between devices, body(): lax.all_gather(up_proj, 'sp', axis=0, tiled=True)  170 us
    all_gather x1, waiting for transfers between devices, body(): lax.all_gather(down_proj, axis_name='sp')  169 us
    reshape x1, local copies, waits for them, and re-layouts, body(): jnp.concatenate(lax.all_gather(down_proj, axis_name='sp'), 1)  21.4 us
    psum x1, waiting for transfers between devices, body(): lax.psum(jnp.dot(attn, out_proj, preferred_element_type=jnp.float32).asty...  19.4 us
    dot_general x1, matrix products, body(): jnp.dot(hidden, jnp.concatenate(lax.all_gather(down_proj, axis_name='sp')...  18.8 us
  transfers between devices with their start and end apart: 6, of which 6 were waited for; matrix products, arithmetic and copies ran while one was open for 7% of the time, Pallas kernels for 0%

profile of v1, /device:TPU:0, one launch (start us, length us, event | category | flops | bytes accessed | tf_op | source)
XLA Modules:
  0.0 471.7 jit_solution(55040648973050308)
XLA Ops:
  7.4 1.3 copy.28
  8.7 1.2 copy.29
  9.9 0.4 multiply_cosine_fusion
  10.3 0.1 fusion.40
  10.5 0.8 pad_maximum_fusion.7
  11.3 5.6 %collective-permute-start = (bf16[2,128,512]{1,2,0:T(8,128)(2,1)}, bf16[2,128,512]{1,2,0:T(8,128)(2,1)}, u32[]{:S(2)}, u32[]{:S(2)}) collective-permute-start(bf16[2,128,512]{1,2,0:T(8,128)(2,1)} %get-tuple-element.15), channel_id=1, source_target_pairs={{0,2},{2,4},{4,6},{6,8},{8,10},{10,12},{12,14},{14,16},{16,18},{18... | collective-permute-start | bytes 786440 | tf_op jit(solution)/shard_map/ppermute | solution.py:17
  16.9 1.3 collective-permute-start.1
  18.3 0.7 abs_compare_fusion
  19.0 0.4 copy.59
  19.4 0.3 fusion.34
  19.7 0.9 copy.36
  20.7 0.1 slice.109
  20.8 0.1 concatenate.36
  20.9 1.3 copy.43
  22.2 0.1 concatenate.37
  22.3 1.2 copy.44
  23.5 0.7 max.25
  24.2 1.0 copy.33
  25.1 0.2 compare_and_fusion
  25.4 2.3 collective-permute-done
  27.7 1.9 collective-permute-done.1
  29.6 1.3 pad_maximum_fusion.5
  30.9 0.1 reshape.217
  31.0 0.3 copy.38
  31.3 0.1 reshape.218
  31.4 0.3 copy.40
  31.8 2.4 fusion
  34.3 2.0 copy-done
  36.4 1.2 fusion.1
  37.7 0.1 reshape.215
  37.9 0.1 reshape.216
  38.1 4.0 fusion.23
  42.0 0.6 copy.46
  42.7 0.6 reshape.209
  43.2 5.1 %convolution_convert_fusion = bf16[384,2048]{1,0:T(8,128)(2,1)} fusion(bf16[384,1024]{1,0:T(8,128)(2,1)S(1)} %reshape.209, bf16[1024,2048]{1,0:T(8,128)(2,1)} %param.18), kind=kOutput, calls=%fused_computation.19 | convolution fusion | flops 1611399168 | bytes 6553600 | tf_op jit(solution)/shard_map/dot_general | solution.py:98
  48.4 0.5 all-gather.6.cloned.1.call-update
  49.0 0.5 all-gather.4.cloned.1.call-update
  49.6 0.2 reduce-scatter.2.cloned.1.call-start
  49.8 19.4 %all-reduce.3.cloned.1.call-done = bf16[384,2048]{1,0:T(8,128)(2,1)} async-done(((bf16[384,2048]{1,0:T(8,128)(2,1)}), bf16[384,2048]{1,0:T(8,128)(2,1)}) %all-reduce.3.cloned.1.call-update) | async-done | bytes 1572880 | tf_op jit(solution)/shard_map/psum | solution.py:97
  69.2 1.8 fusion.2
  71.0 2.3 fusion.6
  73.3 169.4 %all-gather.6.cloned.1.call-done = bf16[65536,128]{1,0:T(8,128)(2,1)} async-done(((bf16[4096,128]{1,0:T(8,128)(2,1)}), bf16[65536,128]{1,0:T(8,128)(2,1)}) %all-gather.6.cloned.1.call-update) | async-done | bytes 16777232 | tf_op jit(solution)/shard_map/all_gather | solution.py:113
  242.7 21.4 %copy.47 = bf16[4096,16,128]{0,2,1:T(8,128)(2,1)} copy(bf16[4096,16,128]{2,0,1:T(8,128)(2,1)} %bitcast.62) | data formatting | bytes 33554432 | tf_op jit(solution)/shard_map/reshape | solution.py:113
  264.1 170.2 %all-gather.4.cloned.1.call-done = bf16[2048,4096]{1,0:T(8,128)(2,1)} async-done(((bf16[128,4096]{1,0:T(8,128)(2,1)}), bf16[2048,4096]{1,0:T(8,128)(2,1)}) %all-gather.4.cloned.1.call-update) | async-done | bytes 16777232 | tf_op jit(solution)/shard_map/all_gather | solution.py:107
  434.3 18.8 %fusion.10 = bf16[384,2048]{1,0:T(8,128)(2,1)} fusion(bf16[4096,2048]{0,1:T(8,128)(2,1)} %bitcast.63, bf16[2048,4096]{1,0:T(8,128)(2,1)} %all-gather.4.cloned.1.call-done, bf16[384,2048]{1,0:T(8,128)(2,1)S(1)} %get-tuple-element.6, f32[2048]{0:T(1024)S(1)} %copy-done.12, f32[384]{0:T(512)S(1)} %add_rsqrt_fusion), kind=kOutput, calls=%fused_computation.18 | convolution fusion | flops 12893552640 | bytes 36709888 | tf_op jit(solution)/shard_map/dot_general | solution.py:111
  453.1 7.4 %reduce-scatter.2.cloned.1.call-done = bf16[192,2048]{1,0:T(8,128)(2,1)} async-done(((bf16[384,2048]{1,0:T(8,128)(2,1)}), bf16[192,2048]{1,0:T(8,128)(2,1)}) %reduce-scatter.2.cloned.1.call-update) | async-done | bytes 786448 | tf_op jit(solution)/shard_map/reduce_scatter | solution.py:116
  460.5 1.4 fusion.12
  461.9 2.4 fusion.15
  (45 shorter events, 0.7 us)
Async XLA Ops:
  7.4 10.8 %copy-start.7 = (s32[6144]{0:T(1024)S(1)}, s32[6144]{0:T(1024)}, u32[]{:S(2)}) copy-start(s32[6144]{0:T(1024)} %param.16) | copy-start | bytes 73732
  7.4 11.6 %copy-start.3 = (bf16[384,1024]{1,0:T(8,128)(2,1)S(1)}, bf16[384,1024]{1,0:T(8,128)(2,1)}, u32[]{:S(2)}) copy-start(bf16[384,1024]{1,0:T(8,128)(2,1)} %param.12) | copy-start | bytes 2359300
  7.4 61.8 %all-reduce.3.cloned.1.call-start = ((), (), s32[]{:S(2)}) async-start(), calls=%async_computation.1 | async-start | bytes 3145728 | tf_op jit(solution)/shard_map/psum | solution.py:97
  10.5 10.2 %copy-start.1 = (bf16[384,512]{1,0:T(8,128)(2,1)S(1)}, bf16[384,512]{1,0:T(8,128)(2,1)}, u32[]{:S(2)}) copy-start(bf16[384,512]{1,0:T(8,128)(2,1)} %param.14) | copy-start | bytes 1179652
  11.3 16.3 %collective-permute-start = (bf16[2,128,512]{1,2,0:T(8,128)(2,1)}, bf16[2,128,512]{1,2,0:T(8,128)(2,1)}, u32[]{:S(2)}, u32[]{:S(2)}) collective-permute-start(bf16[2,128,512]{1,2,0:T(8,128)(2,1)} %get-tuple-element.15), channel_id=1, source_target_pairs={{0,2},{2,4},{4,6},{6,8},{8,10},{10,12},{12,14},{14,16},{16,18},{18... | collective-permute-start | bytes 786440 | tf_op jit(solution)/shard_map/ppermute | solution.py:17
  16.9 12.7 %collective-permute-start.1 = (bf16[2,128,512]{1,2,0:T(8,128)(2,1)S(1)}, bf16[2,128,512]{1,2,0:T(8,128)(2,1)}, u32[]{:S(2)}, u32[]{:S(2)}) collective-permute-start(bf16[2,128,512]{1,2,0:T(8,128)(2,1)S(1)} %get-tuple-element.16), channel_id=1, source_target_pairs={{2,0},{4,2},{6,4},{8,6},{10,8},{12,10},{14,12},{16,14},{18,16},{20... | collective-permute-start | bytes 786440 | tf_op jit(solution)/shard_map/ppermute | solution.py:18
  19.6 3.9 copy-start.11
  20.7 4.5 copy-start.6
  25.4 6.4 %copy-start.4 = (bf16[3,128,4,2,64]{4,1,3,2,0:T(8,128)(2,1)S(1)}, bf16[3,128,4,2,64]{4,1,3,2,0:T(8,128)(2,1)}, u32[]{:S(2)}) copy-start(bf16[3,128,4,2,64]{4,1,3,2,0:T(8,128)(2,1)} %copy.43) | copy-start | bytes 1179652
  31.8 2.5 copy-start.8
  34.2 2.1 copy-start
  36.4 1.7 copy-start.5
  48.4 22.6 %copy-start.2 = (bf16[384,2048]{1,0:T(8,128)(2,1)S(1)}, bf16[384,2048]{1,0:T(8,128)(2,1)}, u32[]{:S(2)}) copy-start(bf16[384,2048]{1,0:T(8,128)(2,1)} %param.17) | copy-start | bytes 4718596
  48.4 22.6 %copy-start.9 = (f32[2048]{0:T(1024)S(1)}, f32[2048]{0:T(1024)}, u32[]{:S(2)}) copy-start(f32[2048]{0:T(1024)} %param.19) | copy-start | bytes 24580
  48.4 194.3 %all-gather.6.cloned.1.call-start = ((), (), s32[]{:S(2)}) async-start(), calls=%async_computation.4 | async-start | bytes 17825792 | tf_op jit(solution)/shard_map/all_gather | solution.py:113
  49.0 385.3 %all-gather.4.cloned.1.call-start = ((), (), s32[]{:S(2)}) async-start(), calls=%async_computation.2 | async-start | bytes 17825792 | tf_op jit(solution)/shard_map/all_gather | solution.py:107
  49.6 410.9 %reduce-scatter.2.cloned.1.call-start = ((), (), s32[]{:S(2)}) async-start(), calls=%async_computation.3 | async-start | bytes 2359296 | tf_op jit(solution)/shard_map/reduce_scatter | solution.py:116
  242.7 191.6 %copy-start.12 = (f32[2048]{0:T(1024)S(1)}, f32[2048]{0:T(1024)}, u32[]{:S(2)}) copy-start(f32[2048]{0:T(1024)} %param.22) | copy-start | bytes 24580
  434.3 27.6 %copy-start.10 = (f32[2048]{0:T(1024)S(1)}, f32[2048]{0:T(1024)}, u32[]{:S(2)}) copy-start(f32[2048]{0:T(1024)} %param.23) | copy-start | bytes 24580
Sparse Core Ops, SparseCore 0:
  48.5 20.6 all-reduce.2
  453.2 7.2 reduce-scatter.1
Sparse Core Ops, SparseCore 1:
  51.6 191.0 all-gather.5
  245.3 188.9 all-gather.3
